TPU v7x, 32 devices: a whole 2x2x4 slice. The times are simulated.
32 devices in a mesh: fs: 8 (over z, x), tp: 4 (over y, core).
Axes of the slice: x: 2, y: 2, z: 4, core: 2. Of those that a mesh axis runs over, the one named last changes fastest.
Arguments:
- inputs: bfloat16 [3072, 2048], P('fs'), may hold values from -6 to 6
- queries: bfloat16 [3072, 2048], P('fs', 'tp'), may hold values from -6 to 6
- keys: bfloat16 [3072, 2048], P('fs', 'tp'), may hold values from -6 to 6
- values: bfloat16 [3072, 2048], P('fs', 'tp'), may hold values from -6 to 6
- head_cot: bfloat16 [3072, 2048], P('fs', 'tp'), may hold values from -6 to 6
- mixing: float32 [16], P('tp'), may hold values from 0.3 to 0.8
- head_gain: float32 [128], replicated, may hold values from 0.1 to 1.9
- factors: bfloat16 [2048, 2, 256], P('fs'), may hold values from -0.375 to 0.375
- moments: float32 [256, 2, 2048], P('fs', None, 'tp'), may hold values from -6 to 6
- weights: float32 [2048, 2, 2048], P('fs', None, 'tp'), may hold values from -6 to 6
Outputs:
- step: float32 [2048, 2, 2048], P('fs', None, 'tp')
- new_moments: float32 [256, 2, 2048], P('fs', None, 'tp')
- copies: bfloat16 [2048, 2, 2048], P(None, None, 'tp')
All inputs are finite; a program needn't handle non-finite values.
Results may differ from a plain program's by a relative error of at most 0.007.
Values may be sent and summed in bfloat16 or wider, within the bound.
A program may use at most 64 MiB of HBM per device.

v0:
```python
import jax
import jax.numpy as jnp
from jax import lax
from jax.sharding import PartitionSpec as P

EPS = 0.05
BETA = 0.9
RATE_BASE = 0.5


def softmax_rows(scores):
    top = jnp.max(scores, axis=-1, keepdims=True)
    expo = jnp.exp(scores - top)
    return expo / jnp.sum(expo, axis=-1, keepdims=True)


def head_grads(query, key_rows, value, upstream, weight_mix, head_gain):
    length = query.shape[0]
    head_dim = query.shape[2]
    factor = head_dim ** (-0.5)
    places = jnp.arange(length)
    causal = places[None, :] <= places[:, None]

    def probs(which):
        scores = (
            jnp.dot(query[:, which], key_rows[:, which].T, preferred_element_type=jnp.float32)
            * factor
        )
        return softmax_rows(jnp.where(causal, scores, -jnp.inf))

    first = probs(0)
    second = probs(1)
    mixed = (first - weight_mix * second).astype(jnp.bfloat16)
    output = jnp.dot(mixed, value, preferred_element_type=jnp.float32)
    inverse = lax.rsqrt(jnp.mean(output * output, axis=-1, keepdims=True) + EPS)
    scaled = head_gain * upstream.astype(jnp.float32)
    d_out = inverse * scaled - output * inverse**3 * jnp.mean(
        output * scaled, axis=-1, keepdims=True
    )
    d_out = d_out.astype(jnp.bfloat16)
    d_value = jnp.dot(mixed.T, d_out, preferred_element_type=jnp.float32).astype(jnp.bfloat16)
    d_mix = jnp.dot(d_out, value.T, preferred_element_type=jnp.float32)
    d_first = (first * (d_mix - jnp.sum(first * d_mix, axis=-1, keepdims=True))).astype(
        jnp.bfloat16
    )
    d_second = (
        -weight_mix * second * (d_mix - jnp.sum(second * d_mix, axis=-1, keepdims=True))
    ).astype(jnp.bfloat16)
    q_first = (
        jnp.dot(d_first, key_rows[:, 0], preferred_element_type=jnp.float32) * factor
    ).astype(jnp.bfloat16)
    q_second = (
        jnp.dot(d_second, key_rows[:, 1], preferred_element_type=jnp.float32) * factor
    ).astype(jnp.bfloat16)
    return (jnp.stack([q_first, q_second], axis=1).reshape(length, 2 * head_dim), d_value)


def per_device(
    inputs, queries, keys, values, head_cot, mixing, head_gain, factors, moments, weights
):
    length = inputs.shape[0]
    heads_here = mixing.shape[0]
    head_width = values.shape[1] // heads_here
    head_dim = head_width // 2
    query_heads = queries.reshape(length, heads_here, 2, head_dim).transpose(1, 0, 2, 3)
    key_heads = keys.reshape(length, heads_here, 2, head_dim).transpose(1, 0, 2, 3)
    value_heads = values.reshape(length, heads_here, head_width).transpose(1, 0, 2)
    upstream_heads = head_cot.reshape(length, heads_here, head_width).transpose(1, 0, 2)

    def one_head(pieces):
        return head_grads(pieces[0], pieces[1], pieces[2], pieces[3], pieces[4], head_gain)

    d_query, d_value = lax.map(
        one_head, (query_heads, key_heads, value_heads, upstream_heads, mixing)
    )
    d_query = d_query.transpose(1, 0, 2).reshape(length, heads_here * head_width)
    d_value = d_value.transpose(1, 0, 2).reshape(length, heads_here * head_width)
    cotangents = jnp.stack([d_query, d_value], axis=1)
    fs_count = lax.axis_size("fs")
    token_factor = (length * fs_count) ** (-0.5)
    rank_here = moments.shape[0]
    cols_here = moments.shape[2]
    factor_wide = factors.astype(jnp.float32)
    whole_factors = lax.all_gather(factors, "fs", axis=0, tiled=True)
    reduced = jnp.einsum("td,dkr->tkr", inputs, whole_factors, preferred_element_type=jnp.float32)
    reduced_upper = reduced.astype(jnp.bfloat16)
    reduced_lower = (reduced - reduced_upper.astype(jnp.float32)).astype(jnp.bfloat16)
    upper_part = jnp.einsum(
        "tkr,tke->rke", reduced_upper, cotangents, preferred_element_type=jnp.float32
    )
    lower_part = jnp.einsum(
        "tkr,tke->rke", reduced_lower, cotangents, preferred_element_type=jnp.float32
    )
    projected = lax.psum_scatter(upper_part + lower_part, "fs", scatter_dimension=0, tiled=True)
    projected = projected * token_factor
    new_moments = BETA * moments + projected
    local_sums = jnp.sum(new_moments * new_moments, axis=(0, 2))
    totals = lax.psum(local_sums, ("fs", "tp"))
    entries = rank_here * fs_count * cols_here * lax.axis_size("tp")
    rate = RATE_BASE / jnp.sqrt(1.0 + totals / entries)
    low_part = jnp.einsum(
        "dkr,rke->dke",
        factor_wide,
        lax.all_gather(new_moments, "fs", axis=0, tiled=True),
        precision=lax.Precision.HIGHEST,
    )
    step = low_part * rate[None, :, None]
    copies = lax.all_gather((weights - step).astype(jnp.bfloat16), "fs", axis=0, tiled=True)
    return (step, new_moments, copies)


def solution(mesh):
    placed = (
        P("fs", None),
        P("fs", "tp"),
        P("fs", "tp"),
        P("fs", "tp"),
        P("fs", "tp"),
        P("tp"),
        P(),
        P("fs", None, None),
        P("fs", None, "tp"),
        P("fs", None, "tp"),
    )
    return jax.shard_map(
        per_device,
        mesh=mesh,
        in_specs=placed,
        out_specs=(P("fs", None, "tp"), P("fs", None, "tp"), P(None, None, "tp")),
        check_vma=False,
    )
```

profile of v0, /device:TPU:0, one launch (start us, length us, event | category | flops | bytes accessed | tf_op | source)
XLA Modules:
  0.0 282.7 jit_solution(10454785109164463003)
XLA Ops:
  7.3 1.8 copy.46
  9.2 1.2 copy.39
  10.4 1.2 copy.40
  11.8 1.2 copy.42
  13.0 21.3 %while.12 = (s32[]{:T(128)}, bf16[4,384,128]{1,2,0:T(8,128)(2,1)S(1)}, bf16[4,384,128]{2,1,0:T(8,128)(2,1)}, bf16[4,384,2,64]{1,3,2,0:T(8,128)(2,1)S(1)}, bf16[4...) while((s32[]{:T(128)}, ...), condition=%wide.region_9.10_spmd, body=%wide.region_0.9_spmd.sunk | while | flops 195525504 | bytes 10978449 | solution.py:73
  13.1 0.6 dynamic_slice.47
  15.2 0.8 subtract_convert_fusion.5
  16.3 1.0 fusion.71
  18.4 0.6 dynamic_slice.47
  20.5 0.8 subtract_convert_fusion.5
  21.6 1.0 fusion.71
  23.7 0.6 dynamic_slice.47
  25.8 0.8 subtract_convert_fusion.5
  26.9 1.0 fusion.71
  29.0 0.6 dynamic_slice.47
  31.2 0.8 subtract_convert_fusion.5
  32.3 1.0 fusion.71
  34.3 1.2 copy.45
  35.6 27.0 %all-gather.4.cloned.1.call-done = bf16[2048,2,256]{2,0,1:T(8,128)(2,1)} async-done(((bf16[256,2,256]{2,0,1:T(8,128)(2,1)}), bf16[2048,2,256]{2,0,1:T(8,128)(2,1)}) %all-gather.4.cloned.1.call-update) | async-done | bytes 2097168 | tf_op jit(solution)/shard_map/all_gather | solution.py:84
  62.6 2.6 fusion.30
  65.2 0.4 fusion.35
  65.6 0.4 fusion.32
  66.1 1.3 copy.47
  67.5 0.6 dynamic-slice
  68.7 75.5 %all-reduce.3.cloned.1.call-done = f32[256,2,512]{2,1,0:T(2,128)} async-done(((f32[256,2,512]{2,1,0:T(2,128)}), f32[256,2,512]{2,1,0:T(2,128)}) %all-reduce.3.cloned.1.call-update) | async-done | bytes 1048592
  144.3 1.8 multiply_reduce_fusion.3
  146.1 1.4 copy.50
  147.6 39.7 %psum.7 = f32[2]{0:T(128)S(1)} all-reduce(f32[2]{0:T(128)S(1)} %get-tuple-element.111), channel_id=1, replica_groups=mesh['fs'=8,'tp'=4] {'fs','tp'}, use_global_device_ids=true, to_apply=%region_12.13 | all-reduce | flops 2 | bytes 16 | tf_op jit(solution)/shard_map/psum | solution.py:98
  187.3 3.5 %subtract_convert_fusion.1 = (bf16[256,2,512]{0,2,1:T(8,128)(2,1)}, f32[256,2,512]{0,2,1:T(8,128)S(1)}) fusion(f32[256,2,512]{0,2,1:T(8,128)} %copy.50, f32[2]{0:T(128)S(1)} %rsqrt_multiply_fusion, bf16[256,2,256]{2,1,0:T(2,128)(2,1)S(1)} %copy-done.1, f32[256,2,512]{2,1,0:T(2,128)} %all-gather.6.cloned.1.call-done), kind=kOutput, calls=%fused_computation.61 | convolution fusion | flops 806092800 | bytes 3932168 | tf_op jit(solution)/shard_map/dkr,rke->dke/dot_general | solution.py:101
  190.8 1.3 copy.51
  192.1 72.9 %all-gather.8.cloned.1.call-done = bf16[2048,2,512]{0,2,1:T(8,128)(2,1)} async-done(((bf16[256,2,512]{0,2,1:T(8,128)(2,1)}), bf16[2048,2,512]{0,2,1:T(8,128)(2,1)}) %all-gather.8.cloned.1.call-update) | async-done | bytes 4194320 | tf_op jit(solution)/shard_map/all_gather | solution.py:108
  265.0 11.1 %copy.52 = bf16[2048,2,512]{2,1,0:T(2,128)(2,1)} copy(bf16[2048,2,512]{0,2,1:T(8,128)(2,1)} %all-gather.8.cloned.1.call-done) | data formatting | bytes 8388608
  (81 shorter events, 9.3 us)
Async XLA Ops:
  7.2 55.4 %copy-start = (bf16[384,2048]{1,0:T(8,128)(2,1)S(1)}, bf16[384,2048]{1,0:T(8,128)(2,1)}, u32[]{:S(2)}) copy-start(bf16[384,2048]{1,0:T(8,128)(2,1)} %param.12) | copy-start | bytes 4718596
  7.2 4.4 %copy-start.3 = (bf16[384,512]{1,0:T(8,128)(2,1)S(1)}, bf16[384,512]{1,0:T(8,128)(2,1)}, u32[]{:S(2)}) copy-start(bf16[384,512]{1,0:T(8,128)(2,1)} %param.15) | copy-start | bytes 1179652
  7.2 5.8 %copy-start.5 = (f32[128]{0:T(128)S(1)}, f32[128]{0:T(128)}, u32[]{:S(2)}) copy-start(f32[128]{0:T(128)} %param.18) | copy-start | bytes 1540
  7.2 5.8 %copy-start.6 = (f32[4]{0:T(128)S(1)}, f32[4]{0:T(128)}, u32[]{:S(2)}) copy-start(f32[4]{0:T(128)} %param.17) | copy-start | bytes 52
  7.2 55.4 %all-gather.4.cloned.1.call-start = ((), (), s32[]{:S(2)}) async-start(), calls=%async_computation | async-start | bytes 2359296 | tf_op jit(solution)/shard_map/all_gather | solution.py:84
  9.1 135.2 %all-reduce.3.cloned.1.call-start = ((), (), s32[]{:S(2)}) async-start(), calls=%async_computation.3 | async-start | bytes 2097152
  66.1 1.4 copy-start.7
  66.1 78.2 %copy-start.4 = (f32[32,2,512]{2,1,0:T(2,128)S(1)}, f32[32,2,512]{2,1,0:T(2,128)}, u32[]{:S(2)}) copy-start(f32[32,2,512]{2,1,0:T(2,128)} %param.20) | copy-start | bytes 393220
  67.4 78.8 %copy-start.2 = (f32[256,2,512]{2,1,0:T(2,128)S(1)}, f32[256,2,512]{2,1,0:T(2,128)}, u32[]{:S(2)}) copy-start(f32[256,2,512]{2,1,0:T(2,128)} %param.21) | copy-start | bytes 3145732
  67.4 119.9 %copy-start.1 = (bf16[256,2,256]{2,1,0:T(2,128)(2,1)S(1)}, bf16[256,2,256]{2,1,0:T(2,128)(2,1)}, u32[]{:S(2)}) copy-start(bf16[256,2,256]{2,1,0:T(2,128)(2,1)} %param.19) | copy-start | bytes 786436
  67.4 119.9 %all-gather.6.cloned.1.call-start = ((), (), s32[]{:S(2)}) async-start(), calls=%async_computation.1 | async-start | bytes 1179648 | tf_op jit(solution)/shard_map/all_gather | solution.py:104
  146.1 118.9 %all-gather.8.cloned.1.call-start = ((), (), s32[]{:S(2)}) async-start(), calls=%async_computation.2 | async-start | bytes 4718592 | tf_op jit(solution)/shard_map/all_gather | solution.py:108
Sparse Core Ops, SparseCore 0:
  10.8 51.7 all-gather.3
  67.5 76.6 all-reduce.2
  147.0 40.0 all-gather.5
  190.9 74.0 all-gather.7
where the time goes:
time: 283 us
  waiting for transfers between devices  176 us (62%)
  blocking collectives  39.7 us (14%)
  local copies, waits for them, and re-layouts  25.2 us (9%)
  matrix products  18.3 us (6%)
  between operations  14.6 us (5%)
  other arithmetic  6.28 us (2%)
    unnamed x5, waiting for transfers between devices  75.6 us
    all_gather x1, waiting for transfers between devices, per_device(): lax.all_gather((weights - step).astype(jnp.bfloat16), 'fs', axis=0, tiled...  72.9 us
    psum x1, blocking collectives, per_device(): totals = lax.psum(local_sums, ('fs', 'tp'))  39.7 us
    all_gather x1, waiting for transfers between devices, per_device(): whole_factors = lax.all_gather(factors, 'fs', axis=0, tiled=True)  27 us
    unnamed x25, local copies, waits for them, and re-layouts  20.1 us
  transfers between devices with their start and end apart: 4, of which 3 were waited for; matrix products, arithmetic and copies ran while one was open for 10% of the time, Pallas kernels for 0%

commit v1 on v0

--- a/solution.py
+++ b/solution.py
@@ -81,8 +81,35 @@
     rank_here = moments.shape[0]
     cols_here = moments.shape[2]
     factor_wide = factors.astype(jnp.float32)
-    whole_factors = lax.all_gather(factors, "fs", axis=0, tiled=True)
-    reduced = jnp.einsum("td,dkr->tkr", inputs, whole_factors, preferred_element_type=jnp.float32)
+    size, index, span = (lax.axis_size("fs"), lax.axis_index("fs"), factors.shape[0])
+    upward = [(i, (i + 1) % size) for i in range(size)]
+    downward = [(i, (i - 1) % size) for i in range(size)]
+    middle = size // 2
+    from_left = from_right = factors
+    reduced = jnp.einsum(
+        "td,dkr->tkr",
+        lax.dynamic_slice_in_dim(inputs, index * span, factors.shape[0], axis=1),
+        factors,
+        preferred_element_type=jnp.float32,
+    )
+    for k in range(1, middle + 1):
+        from_left = lax.ppermute(from_left, "fs", upward)
+        if k < size - middle:
+            from_right = lax.ppermute(from_right, "fs", downward)
+            reduced = reduced + jnp.einsum(
+                "td,dkr->tkr",
+                lax.dynamic_slice_in_dim(
+                    inputs, (index + k) % size * span, from_right.shape[0], axis=1
+                ),
+                from_right,
+                preferred_element_type=jnp.float32,
+            )
+        reduced = reduced + jnp.einsum(
+            "td,dkr->tkr",
+            lax.dynamic_slice_in_dim(inputs, (index - k) % size * span, from_left.shape[0], axis=1),
+            from_left,
+            preferred_element_type=jnp.float32,
+        )
     reduced_upper = reduced.astype(jnp.bfloat16)
     reduced_lower = (reduced - reduced_upper.astype(jnp.float32)).astype(jnp.bfloat16)
     upper_part = jnp.einsum(

time: 283 us -> 299 us (1.057)
  starting transfers between devices: 0.16 us -> 16.8 us
  waiting for transfers between devices: 176 us -> 172 us
    all_gather x1 -> x0, waiting for transfers between devices: 27 us -> none  [per_device(): whole_factors = lax.all_gather(factors, 'fs', axis=0, tiled=True)]
    ppermute x0 -> x7, waiting for transfers between devices: none -> 23.1 us  [the longest x4 20.3 us: per_device(): from_left = lax.ppermute(from_left, 'fs', upward)]
    ppermute x0 -> x7, starting transfers between devices: none -> 16.7 us  [the longest x3 16.7 us: per_device(): from_right = lax.ppermute(from_right, 'fs', downward)]
    unnamed x25 -> x29, local copies, waits for them, and re-layouts: 20.1 us -> 19.2 us
    unnamed x5 -> x4, waiting for transfers between devices: 75.6 us -> 75.6 us
  transfers between devices with their start and end apart: 4 -> 10, of which waited for: 3 -> 5; matrix products, arithmetic and copies ran while one was open for 10% -> 11% of each run, Pallas kernels for 0% -> 0%
where the time goes in v1:
time: 299 us
  waiting for transfers between devices  172 us (58%)
  blocking collectives  39.7 us (13%)
  local copies, waits for them, and re-layouts  27 us (9%)
  matrix products  19.8 us (7%)
  starting transfers between devices  16.8 us (6%)
  between operations  14.7 us (5%)
  other arithmetic  6.31 us (2%)
    unnamed x4, waiting for transfers between devices  75.6 us
    all_gather x1, waiting for transfers between devices, per_device(): lax.all_gather((weights - step).astype(jnp.bfloat16), 'fs', axis=0, tiled...  72.9 us
    psum x1, blocking collectives, per_device(): totals = lax.psum(local_sums, ('fs', 'tp'))  39.7 us
    ppermute x4, waiting for transfers between devices, per_device(): from_left = lax.ppermute(from_left, 'fs', upward)  20.3 us
    unnamed x29, local copies, waits for them, and re-layouts  19.2 us
    ppermute x3, starting transfers between devices, per_device(): from_right = lax.ppermute(from_right, 'fs', downward)  16.7 us
  transfers between devices with their start and end apart: 10, of which 5 were waited for; matrix products, arithmetic and copies ran while one was open for 11% of the time, Pallas kernels for 0%

profile of v1, /device:TPU:0, one launch (start us, length us, event | category | flops | bytes accessed | tf_op | source)
XLA Modules:
  0.0 298.7 jit_solution(14896907841881317486)
XLA Ops:
  7.2 1.8 copy.50
  9.1 6.0 %collective-permute-start = (bf16[256,2,256]{2,0,1:T(8,128)(2,1)}, bf16[256,2,256]{2,0,1:T(8,128)(2,1)}, u32[]{:S(2)}, u32[]{:S(2)}) collective-permute-start(bf16[256,2,256]{2,0,1:T(8,128)(2,1)} %copy.50), channel_id=1, source_target_pairs={{0,28},{4,0},{8,4},{12,8},{16,12},{20,16},{24,20},{28,24},{1,29},{... | collective-permute-start | bytes 786440 | tf_op jit(solution)/shard_map/ppermute | solution.py:98
  15.1 1.2 copy.43
  16.8 1.2 copy.46
  18.0 24.0 %while.12 = (s32[]{:T(128)}, bf16[4,384,128]{1,2,0:T(8,128)(2,1)}, bf16[4,384,128]{2,1,0:T(8,128)(2,1)}, bf16[4,384,2,64]{1,3,2,0:T(8,128)(2,1)S(1)}, bf16[4,384...) while((s32[]{:T(128)}, bf16[4,384,128]{1,2,0:T(8,128)(2,1)}, ...), condition=%wide.region_9.10_spmd, body=%wide.region_0.9_spmd.sunk | while | flops 195525504 | bytes 10978449 | solution.py:73
  20.2 0.8 subtract_convert_fusion.5
  21.3 1.0 fusion.105
  23.4 0.7 constant_dynamic-update-slice_fusion.2
  26.2 0.8 subtract_convert_fusion.5
  27.3 1.0 fusion.105
  29.4 0.7 constant_dynamic-update-slice_fusion.2
  32.2 0.8 subtract_convert_fusion.5
  33.3 1.0 fusion.105
  38.2 0.8 subtract_convert_fusion.5
  39.3 1.0 fusion.105
  42.0 1.2 copy.49
  43.6 4.8 %collective-permute-start.2 = (bf16[256,2,256]{2,0,1:T(8,128)(2,1)}, bf16[256,2,256]{2,0,1:T(8,128)(2,1)S(1)}, u32[]{:S(2)}, u32[]{:S(2)}) collective-permute-start(bf16[256,2,256]{2,0,1:T(8,128)(2,1)} %collective-permute-done), channel_id=1, source_target_pairs={{0,28},{4,0},{8,4},{12,8},{16,12},{20,16},{24,20},{28,24},{1,29},{... | collective-permute-start | bytes 786440 | tf_op jit(solution)/shard_map/ppermute | solution.py:98
  48.4 1.2 convolution_add_fusion.5
  49.6 1.2 convolution_add_fusion.4
  50.8 2.8 collective-permute-done.2
  53.7 5.9 %collective-permute-start.4 = (bf16[256,2,256]{2,0,1:T(8,128)(2,1)S(1)}, bf16[256,2,256]{2,0,1:T(8,128)(2,1)S(1)}, u32[]{:S(2)}, u32[]{:S(2)}) collective-permute-start(bf16[256,2,256]{2,0,1:T(8,128)(2,1)S(1)} %collective-permute-done.2), channel_id=1, source_target_pairs={{0,28},{4,0},{8,4},{12,8},{16,12},{20,16},{24,20},{28,24},{1,29},{... | collective-permute-start | bytes 786440 | tf_op jit(solution)/shard_map/ppermute | solution.py:98
  60.1 9.6 %collective-permute-done.5 = bf16[256,2,256]{2,0,1:T(8,128)(2,1)S(1)} collective-permute-done((bf16[256,2,256]{2,0,1:T(8,128)(2,1)S(1)}, bf16[256,2,256]{2,0,1:T(8,128)(2,1)S(1)}, u32[]{:S(2)}, u32[]{:S(2)}) %collective-permute-start.5) | collective-permute-done | bytes 262176 | tf_op jit(solution)/shard_map/ppermute | solution.py:96
  70.3 10.6 %collective-permute-done.6 = bf16[256,2,256]{2,0,1:T(8,128)(2,1)S(1)} collective-permute-done((bf16[256,2,256]{2,0,1:T(8,128)(2,1)S(1)}, bf16[256,2,256]{2,0,1:T(8,128)(2,1)S(1)}, u32[]{:S(2)}, u32[]{:S(2)}) %collective-permute-start.6) | collective-permute-done | bytes 262176 | tf_op jit(solution)/shard_map/ppermute | solution.py:96
  82.1 1.3 copy.53
  84.8 75.5 %all-reduce.3.cloned.1.call-done = f32[256,2,512]{2,1,0:T(2,128)} async-done(((f32[256,2,512]{2,1,0:T(2,128)}), f32[256,2,512]{2,1,0:T(2,128)}) %all-reduce.3.cloned.1.call-update) | async-done | bytes 1048592
  160.3 1.8 multiply_reduce_fusion.3
  162.2 1.4 copy.56
  163.6 39.7 %psum.7 = f32[2]{0:T(128)S(1)} all-reduce(f32[2]{0:T(128)S(1)} %get-tuple-element.111), channel_id=1, replica_groups=mesh['fs'=8,'tp'=4] {'fs','tp'}, use_global_device_ids=true, to_apply=%region_12.13 | all-reduce | flops 2 | bytes 16 | tf_op jit(solution)/shard_map/psum | solution.py:125
  203.4 3.4 %subtract_convert_fusion.1 = (bf16[256,2,512]{0,2,1:T(8,128)(2,1)}, f32[256,2,512]{0,2,1:T(8,128)S(1)}) fusion(f32[256,2,512]{0,2,1:T(8,128)} %copy.56, f32[2]{0:T(128)S(1)} %rsqrt_multiply_fusion, bf16[256,2,256]{2,1,0:T(2,128)(2,1)S(1)} %copy-done.1, f32[256,2,512]{2,1,0:T(2,128)} %all-gather.3.cloned.1.call-done), kind=kOutput, calls=%fused_computation.66 | convolution fusion | flops 806092800 | bytes 3932168 | tf_op jit(solution)/shard_map/dkr,rke->dke/dot_general | solution.py:128
  206.8 1.3 copy.57
  208.1 72.9 %all-gather.5.cloned.1.call-done = bf16[2048,2,512]{0,2,1:T(8,128)(2,1)} async-done(((bf16[256,2,512]{0,2,1:T(8,128)(2,1)}), bf16[2048,2,512]{0,2,1:T(8,128)(2,1)}) %all-gather.5.cloned.1.call-update) | async-done | bytes 4194320 | tf_op jit(solution)/shard_map/all_gather | solution.py:135
  281.0 11.1 %copy.58 = bf16[2048,2,512]{2,1,0:T(2,128)(2,1)} copy(bf16[2048,2,512]{0,2,1:T(8,128)(2,1)} %all-gather.5.cloned.1.call-done) | data formatting | bytes 8388608
  (103 shorter events, 16.3 us)
Async XLA Ops:
  7.2 36.1 %copy-start = (bf16[384,2048]{1,0:T(8,128)(2,1)S(1)}, bf16[384,2048]{1,0:T(8,128)(2,1)}, u32[]{:S(2)}) copy-start(bf16[384,2048]{1,0:T(8,128)(2,1)} %param.12) | copy-start | bytes 4718596
  7.2 9.1 %copy-start.4 = (bf16[384,512]{1,0:T(8,128)(2,1)S(1)}, bf16[384,512]{1,0:T(8,128)(2,1)}, u32[]{:S(2)}) copy-start(bf16[384,512]{1,0:T(8,128)(2,1)} %param.14) | copy-start | bytes 1179652
  7.2 9.4 %copy-start.5 = (bf16[384,512]{1,0:T(8,128)(2,1)S(1)}, bf16[384,512]{1,0:T(8,128)(2,1)}, u32[]{:S(2)}) copy-start(bf16[384,512]{1,0:T(8,128)(2,1)} %param.15) | copy-start | bytes 1179652
  7.2 153.1 %all-reduce.3.cloned.1.call-start = ((), (), s32[]{:S(2)}) async-start(), calls=%async_computation.2 | async-start | bytes 2097152
  9.1 34.5 %collective-permute-start = (bf16[256,2,256]{2,0,1:T(8,128)(2,1)}, bf16[256,2,256]{2,0,1:T(8,128)(2,1)}, u32[]{:S(2)}, u32[]{:S(2)}) collective-permute-start(bf16[256,2,256]{2,0,1:T(8,128)(2,1)} %copy.50), channel_id=1, source_target_pairs={{0,28},{4,0},{8,4},{12,8},{16,12},{20,16},{24,20},{28,24},{1,29},{... | collective-permute-start | bytes 786440 | tf_op jit(solution)/shard_map/ppermute | solution.py:98
  15.1 33.3 %collective-permute-start.1 = (bf16[256,2,256]{2,0,1:T(8,128)(2,1)}, bf16[256,2,256]{2,0,1:T(8,128)(2,1)}, u32[]{:S(2)}, u32[]{:S(2)}) collective-permute-start(bf16[256,2,256]{2,0,1:T(8,128)(2,1)} %copy.50), channel_id=1, source_target_pairs={{0,4},{4,8},{8,12},{12,16},{16,20},{20,24},{24,28},{28,0},{1,5},{5... | collective-permute-start | bytes 786440 | tf_op jit(solution)/shard_map/ppermute | solution.py:96
  15.1 2.9 copy-start.7
  15.1 2.9 copy-start.8
  18.0 25.3 %copy-start.1 = (bf16[256,2,256]{2,1,0:T(2,128)(2,1)S(1)}, bf16[256,2,256]{2,1,0:T(2,128)(2,1)}, u32[]{:S(2)}) copy-start(bf16[256,2,256]{2,1,0:T(2,128)(2,1)} %param.19) | copy-start | bytes 786436
  43.6 10.1 %collective-permute-start.2 = (bf16[256,2,256]{2,0,1:T(8,128)(2,1)}, bf16[256,2,256]{2,0,1:T(8,128)(2,1)S(1)}, u32[]{:S(2)}, u32[]{:S(2)}) collective-permute-start(bf16[256,2,256]{2,0,1:T(8,128)(2,1)} %collective-permute-done), channel_id=1, source_target_pairs={{0,28},{4,0},{8,4},{12,8},{16,12},{20,16},{24,20},{28,24},{1,29},{... | collective-permute-start | bytes 786440 | tf_op jit(solution)/shard_map/ppermute | solution.py:98
  48.3 11.2 %collective-permute-start.3 = (bf16[256,2,256]{2,0,1:T(8,128)(2,1)}, bf16[256,2,256]{2,0,1:T(8,128)(2,1)S(1)}, u32[]{:S(2)}, u32[]{:S(2)}) collective-permute-start(bf16[256,2,256]{2,0,1:T(8,128)(2,1)} %collective-permute-done.1), channel_id=1, source_target_pairs={{0,4},{4,8},{8,12},{12,16},{16,20},{20,24},{24,28},{28,0},{1,5},{5... | collective-permute-start | bytes 786440 | tf_op jit(solution)/shard_map/ppermute | solution.py:96
  53.7 16.4 %collective-permute-start.4 = (bf16[256,2,256]{2,0,1:T(8,128)(2,1)S(1)}, bf16[256,2,256]{2,0,1:T(8,128)(2,1)S(1)}, u32[]{:S(2)}, u32[]{:S(2)}) collective-permute-start(bf16[256,2,256]{2,0,1:T(8,128)(2,1)S(1)} %collective-permute-done.2), channel_id=1, source_target_pairs={{0,28},{4,0},{8,4},{12,8},{16,12},{20,16},{24,20},{28,24},{1,29},{... | collective-permute-start | bytes 786440 | tf_op jit(solution)/shard_map/ppermute | solution.py:98
  59.6 10.2 %collective-permute-start.5 = (bf16[256,2,256]{2,0,1:T(8,128)(2,1)S(1)}, bf16[256,2,256]{2,0,1:T(8,128)(2,1)S(1)}, u32[]{:S(2)}, u32[]{:S(2)}) collective-permute-start(bf16[256,2,256]{2,0,1:T(8,128)(2,1)S(1)} %collective-permute-done.3), channel_id=1, source_target_pairs={{0,4},{4,8},{8,12},{12,16},{16,20},{20,24},{24,28},{28,0},{1,5},{5... | collective-permute-start | bytes 786440 | tf_op jit(solution)/shard_map/ppermute | solution.py:96
  69.8 11.2 %collective-permute-start.6 = (bf16[256,2,256]{2,0,1:T(8,128)(2,1)S(1)}, bf16[256,2,256]{2,0,1:T(8,128)(2,1)S(1)}, u32[]{:S(2)}, u32[]{:S(2)}) collective-permute-start(bf16[256,2,256]{2,0,1:T(8,128)(2,1)S(1)} %collective-permute-done.5), channel_id=1, source_target_pairs={{0,4},{4,8},{8,12},{12,16},{16,20},{20,24},{24,28},{28,0},{1,5},{5... | collective-permute-start | bytes 786440 | tf_op jit(solution)/shard_map/ppermute | solution.py:96
  70.3 10.9 %copy-start.2 = (bf16[4,384,128]{1,2,0:T(8,128)(2,1)S(1)}, bf16[4,384,128]{1,2,0:T(8,128)(2,1)}, u32[]{:S(2)}) copy-start(bf16[4,384,128]{1,2,0:T(8,128)(2,1)} %get-tuple-element.51) | copy-start | bytes 1179652
  82.1 1.4 copy-start.9
  82.1 78.2 %copy-start.6 = (f32[32,2,512]{2,1,0:T(2,128)S(1)}, f32[32,2,512]{2,1,0:T(2,128)}, u32[]{:S(2)}) copy-start(f32[32,2,512]{2,1,0:T(2,128)} %param.20) | copy-start | bytes 393220
  83.4 78.7 %copy-start.3 = (f32[256,2,512]{2,1,0:T(2,128)S(1)}, f32[256,2,512]{2,1,0:T(2,128)}, u32[]{:S(2)}) copy-start(f32[256,2,512]{2,1,0:T(2,128)} %param.21) | copy-start | bytes 3145732
  83.5 119.9 %all-gather.3.cloned.1.call-start = ((), (), s32[]{:S(2)}) async-start(), calls=%async_computation | async-start | bytes 1179648 | tf_op jit(solution)/shard_map/all_gather | solution.py:131
  162.1 118.9 %all-gather.5.cloned.1.call-start = ((), (), s32[]{:S(2)}) async-start(), calls=%async_computation.1 | async-start | bytes 4718592 | tf_op jit(solution)/shard_map/all_gather | solution.py:135
Sparse Core Ops, SparseCore 0:
  83.6 76.6 all-reduce.2
  163.0 40.0 all-gather.2
  207.0 74.0 all-gather.4
